TPU v7x, 768 devices: a whole 4x8x12 slice. The times are simulated.
768 devices in a mesh: ep: 48 (over z, x), tp: 16 (over y, core).
Axes of the slice: x: 4, y: 8, z: 12, core: 2. Of those that a mesh axis runs over, the one named last changes fastest.
Arguments:
- tokens: bfloat16 [6144, 2048], P('ep', 'tp'), may hold values from -20 to 20
- routing: int32 [6144, 2], P('ep'), may hold values from 0 to 47, all different within a row; in each aligned block of 128 rows (0 to 127, 128 to 255, ...) at most 8 rows name the same one
- gate_weights: bfloat16 [6144, 2], P('ep'), may hold values from 0 to 1, as said below
- cotangent: bfloat16 [6144, 2048], P('ep', 'tp'), may hold values from -3 to 3
- expert_gate: bfloat16 [48, 2048, 3072], P('ep', None, 'tp'), may hold values from -3 to 3
- expert_up: bfloat16 [48, 2048, 3072], P('ep', None, 'tp'), may hold values from -3 to 3
- expert_down: bfloat16 [48, 3072, 2048], P('ep', 'tp'), may hold values from -0.109375 to 0.109375
- router: bfloat16 [2048, 48], replicated, may hold values from -0.125 to 0.125
Outputs:
- token_grad: float32 [6144, 2048], P('ep', 'tp')
- gate_grad: float32 [6144, 2], P('ep')
- gate_proj_grad: bfloat16 [48, 2048, 3072], P('ep', None, 'tp')
- up_proj_grad: bfloat16 [48, 2048, 3072], P('ep', None, 'tp')
- down_proj_grad: bfloat16 [48, 3072, 2048], P('ep', 'tp')
- router_grad: float32 [48, 2048], P('ep', 'tp')
- gate_row_square: float32 [48, 2048], P('ep')
- up_row_square: float32 [48, 2048], P('ep')
- down_row_square: float32 [48, 3072], P('ep', 'tp')
Inputs may be any that keep to these rules, and one draw needn't show every extreme that they name: `routing`: each token names 2 different experts. Among the 128 rows of one device no expert is named more than 8 times; some device reaches 8. `gate_weights`: each row is positive and sums to one up to rounding.
All inputs are finite; a program needn't handle non-finite values.
Results may differ from a plain program's by a relative error of at most 0.015.
Values may be sent and summed in bfloat16 or wider, within the bound.
A program may use at most 32 MiB of HBM per device.

v0:
```python
import jax
import jax.numpy as jnp
from jax import lax
from jax.sharding import PartitionSpec as P


def side_by_side(arrays, axis, split_dim, concat_dim, along):
    columns = [a.reshape(*a.shape[:along], -1) for a in arrays]
    both = jnp.concatenate(columns, axis=along)
    out, at, done = (
        lax.all_to_all(both, axis, split_axis=split_dim, concat_axis=concat_dim, tiled=True),
        0,
        [],
    )
    for a, column in zip(arrays, columns):
        section = out[..., at : at + column.shape[along]]
        done.append(section.reshape(*section.shape[:along], *a.shape[along:]))
        at += column.shape[along]
    return tuple(done)


def sent_together(arrays, axis, dim, along):
    ends, at = ([], 0)
    for a in arrays[:-1]:
        at += a.shape[along]
        ends.append(at)
    both = jnp.concatenate(arrays, axis=along)
    return tuple(jnp.split(lax.all_gather(both, axis, axis=dim, tiled=True), ends, axis=along))


def sent_to_all(value, axis):
    copies = jnp.broadcast_to(value, (lax.axis_size(axis), *value.shape))
    return lax.all_to_all(copies, axis, split_axis=0, concat_axis=0, tiled=True)


def of_everyone(value, axis):
    everything = sent_to_all(value, axis)
    return jnp.sum(everything, axis=0)


def together(arrays, axis):
    ends = [0]
    for a in arrays:
        ends.append(ends[-1] + a.size)
    so_far = of_everyone(jnp.concatenate([a.ravel() for a in arrays]), axis)
    return tuple((so_far[b:e].reshape(a.shape) for a, b, e in zip(arrays, ends, ends[1:])))


def cut_along(value, dim, peers):
    shape = value.shape
    tiles = value.reshape(*shape[:dim], peers, shape[dim] // peers, *shape[dim + 1 :])
    return jnp.moveaxis(tiles, dim, 0)


def sum_at_owner(value, axis, dim):
    tiles = cut_along(value, dim, lax.axis_size(axis))
    arrived = lax.all_to_all(tiles, axis, split_axis=0, concat_axis=0, tiled=True)
    return arrived.astype(jnp.float32).sum(axis=0)


def sent_together_2(arrays, axis, split_dim, concat_dim, along):
    widths = [a.shape[along] for a in arrays]
    both = jnp.concatenate(arrays, axis=along)
    out = lax.all_to_all(both, axis, split_axis=split_dim, concat_axis=concat_dim, tiled=True)
    return tuple(jnp.split(out, [sum(widths[:k]) for k in range(1, len(widths))], axis=along))


def sent_and_summed(value, axis, dim):
    peers = lax.axis_size(axis)
    tiles = lax.all_to_all(cut_along(value, dim, peers), axis, 0, 0, tiled=True)
    return jnp.sum(tiles, axis=0)


def matmul_tn(left_side, right_side):
    return lax.dot_general(
        left_side, right_side, (((0,), (0,)), ((), ())), preferred_element_type=jnp.float32
    )


def matmul_nt(left_side, right_side):
    return lax.dot_general(
        left_side, right_side, (((1,), (1,)), ((), ())), preferred_element_type=jnp.float32
    )


def slot_table(routing, experts, capacity):
    flat_routes = routing.reshape(-1)
    labels = lax.broadcasted_iota(jnp.int32, (flat_routes.shape[0], experts), 1)
    hit_mask = (flat_routes[:, None] == labels).astype(jnp.int32)
    ranking = jnp.cumsum(hit_mask, axis=0) - 1
    position = jnp.sum(hit_mask * ranking, axis=1)
    slot_id = flat_routes * capacity + position
    slot_index = lax.broadcasted_iota(jnp.int32, (experts * capacity, flat_routes.shape[0]), 0)
    return slot_index == slot_id[None, :]


def shards(tokens, routing, gate_weights, cotangent, expert_gate, expert_up, expert_down, router):
    tok_rows, local_width = tokens.shape
    top_count = routing.shape[1]
    experts = router.shape[1]
    n_tp = lax.axis_size("tp")
    capacity = 3 * top_count * tok_rows // (2 * experts)
    slot_count = experts * capacity
    matches = slot_table(routing, experts, capacity)
    by_token = jnp.any(matches.reshape(slot_count, tok_rows, top_count), axis=2).astype(
        jnp.bfloat16
    )
    input_send = jnp.dot(by_token, tokens, preferred_element_type=jnp.float32).astype(jnp.bfloat16)
    tangent_send = jnp.dot(by_token, cotangent, preferred_element_type=jnp.float32).astype(
        jnp.bfloat16
    )
    weight_flat = gate_weights.reshape(-1).astype(jnp.float32)
    weight_send = jnp.sum(jnp.where(matches, weight_flat[None, :], 0.0), axis=1).astype(
        jnp.bfloat16
    )
    input_slots, tangent_slots, weight_slots = side_by_side(
        (
            input_send.reshape(experts, capacity, local_width),
            tangent_send.reshape(experts, capacity, local_width),
            weight_send.reshape(experts, capacity),
        ),
        "ep",
        0,
        0,
        2,
    )
    input_slots = input_slots.reshape(slot_count, local_width)
    tangent_slots = tangent_slots.reshape(slot_count, local_width)
    slot_weight = weight_slots.reshape(slot_count, 1).astype(jnp.float32)
    gate_matrix = expert_gate[0]
    up_matrix = expert_up[0]
    down_matrix = expert_down[0]
    hidden_local = gate_matrix.shape[1]
    full_input, full_tangent = sent_together((input_slots, tangent_slots), "tp", 1, 0)
    pre_gate = jnp.dot(full_input, gate_matrix, preferred_element_type=jnp.float32)
    pre_up = jnp.dot(full_input, up_matrix, preferred_element_type=jnp.float32)
    back_proj = matmul_nt(full_tangent, down_matrix)
    sigmoid_gate = jax.nn.sigmoid(pre_gate)
    active = pre_gate * sigmoid_gate
    hidden = active * pre_up
    slot_part = jnp.sum(hidden * back_proj, axis=1)
    scaled = (slot_weight * hidden).astype(jnp.bfloat16)
    hidden_grad = slot_weight * back_proj
    gate_pre_grad = (
        hidden_grad * pre_up * sigmoid_gate * (1.0 + pre_gate * (1.0 - sigmoid_gate))
    ).astype(jnp.bfloat16)
    up_pre_grad = (hidden_grad * active).astype(jnp.bfloat16)
    gate_sum = matmul_tn(full_input, gate_pre_grad)
    up_sum = matmul_tn(full_input, up_pre_grad)
    down_sum = matmul_tn(scaled, full_tangent)
    unit_count = hidden_local * n_tp
    slot_gate_grad, gate_square, up_square = together(
        (slot_part, jnp.sum(gate_sum * gate_sum, axis=1), jnp.sum(up_sum * up_sum, axis=1)), "tp"
    )
    slot_grad = sum_at_owner(
        (matmul_nt(gate_matrix, gate_pre_grad) + matmul_nt(up_matrix, up_pre_grad)).astype(
            jnp.bfloat16
        ),
        "tp",
        0,
    )
    back_rows, back_gate = tuple(
        (
            part.astype(jnp.float32)
            for part in sent_together_2(
                (
                    slot_grad.reshape(local_width, experts, capacity).astype(jnp.bfloat16),
                    slot_gate_grad.reshape(1, experts, capacity).astype(jnp.bfloat16),
                ),
                "ep",
                1,
                1,
                0,
            )
        )
    )
    back_flat = back_rows.reshape(local_width, slot_count)
    token_part = lax.dot_general(
        by_token.astype(jnp.float32),
        back_flat,
        (((0,), (1,)), ((), ())),
        precision=lax.Precision.HIGHEST,
        preferred_element_type=jnp.float32,
    )
    gate_grad = jnp.sum(jnp.where(matches, back_gate.reshape(slot_count, 1), 0.0), axis=0).reshape(
        tok_rows, top_count
    )
    weights_f = gate_weights.astype(jnp.float32)
    mixed_term = jnp.sum(weights_f * gate_grad, axis=1, keepdims=True)
    logit_grad = weights_f * (gate_grad - mixed_term)
    labels = lax.broadcasted_iota(jnp.int32, (1, 1, experts), 2)
    signal = jnp.sum(
        jnp.where(routing[:, :, None] == labels, logit_grad[:, :, None], 0.0), axis=1
    ).astype(jnp.bfloat16)
    router_term = matmul_tn(signal, tokens)
    router_grad = sent_and_summed(router_term, "ep", 0)
    router_cols = lax.dynamic_slice_in_dim(
        router, lax.axis_index("tp") * local_width, local_width, 0
    )
    token_grad = token_part + matmul_nt(signal, router_cols)
    return (
        token_grad,
        gate_grad,
        gate_sum.astype(jnp.bfloat16)[None],
        up_sum.astype(jnp.bfloat16)[None],
        down_sum.astype(jnp.bfloat16)[None],
        router_grad,
        (gate_square / unit_count)[None, :],
        (up_square / unit_count)[None, :],
        jnp.mean(down_sum * down_sum, axis=1)[None, :],
    )


def solution(mesh):
    in_specs = (
        P("ep", "tp"),
        P("ep", None),
        P("ep", None),
        P("ep", "tp"),
        P("ep", None, "tp"),
        P("ep", None, "tp"),
        P("ep", "tp", None),
        P(),
    )
    out_specs = (
        P("ep", "tp"),
        P("ep", None),
        P("ep", None, "tp"),
        P("ep", None, "tp"),
        P("ep", "tp", None),
        P("ep", "tp"),
        P("ep", None),
        P("ep", None),
        P("ep", "tp"),
    )
    return jax.shard_map(shards, mesh=mesh, in_specs=in_specs, out_specs=out_specs, check_vma=False)
```

profile of v0, /device:TPU:1, one launch (start us, length us, event | category | flops | bytes accessed | tf_op | source)
XLA Modules:
  0.0 215.6 jit_solution(9321054921847335403)
XLA Ops:
  7.2 0.0 copy-start
  7.2 0.0 all-gather.2.cloned.1.call-start
  7.2 0.9 copy.80
  8.1 0.1 eq.44
  8.2 0.1 eq.47
  8.4 0.6 reduce-window.6
  9.0 0.2 slice_reduce_fusion
  9.2 0.1 fusion.27
  9.3 0.1 reduce_sum.116
  9.5 0.1 copy.83
  9.5 0.7 multiply_add_fusion.1
  10.3 0.8 copy.84
  11.1 0.1 reshape.152
  11.2 0.2 select_reduce_fusion.1
  11.4 0.2 convert_element_type.119
  11.6 0.9 fusion.6
  12.5 0.9 fusion.5
  13.5 36.2 %all_to_all.26 = bf16[48,8,257]{2,1,0:T(8,128)(2,1)S(1)} all-to-all(bf16[48,8,257]{2,1,0:T(8,128)(2,1)S(1)} %pad_maximum_fusion), channel_id=1, replica_groups=mesh['ep'=48,'tp'=16] {'ep'}, dimensions={0} | all-to-all | bytes 394752 | tf_op jit(solution)/shard_map/all_to_all | solution.py:11
  49.8 0.0 copy-start.2
  49.8 0.7 pad_maximum_fusion.1
  50.5 0.0 all-gather.2.cloned.1.call-update
  50.5 0.1 convert_reduce_fusion.1
  50.6 0.1 reshape.153
  50.7 45.6 %all-gather.2.cloned.1.call-done = bf16[768,2048]{1,0:T(8,128)(2,1)} async-done(((bf16[768,128]{1,0:T(8,128)(2,1)}), bf16[768,2048]{1,0:T(8,128)(2,1)}) %all-gather.2.cloned.1.call-update) | async-done | bytes 3145744 | tf_op jit(solution)/shard_map/all_gather | solution.py:28
  96.3 0.0 copy-done
  96.3 2.2 %fusion.11 = f32[384,192]{0,1:T(8,128)S(1)} fusion(bf16[768,2048]{1,0:T(8,128)(2,1)} %all-gather.2.cloned.1.call-done, bf16[1,2048,192]{1,2,0:T(8,128)(2,1)S(1)} %copy-done), kind=kOutput, calls=%fused_computation.19 | convolution fusion | flops 301989888 | bytes 2654208 | tf_op jit(solution)/shard_map/dot_general | solution.py:135
  98.5 0.0 copy-done.2
  98.6 0.1 copy-done.1
  98.7 0.7 fusion.13
  99.4 0.4 copy-done.7
  99.8 0.8 multiply_reduce_fusion.3
  100.6 0.6 fusion.7
  101.2 1.8 convert_bitcast_fusion.1
  103.0 0.9 broadcast_in_dim.65
  103.8 4.5 %all-to-all-start.2 = ((f32[16,1,4480]{2,1,0:T(1,128)}), f32[16,1,4480]{2,1,0:T(1,128)S(1)}, u32[]{:S(2)}, u32[]{:S(2)}) async-start(f32[16,1,4480]{2,1,0:T(1,128)} %broadcast_in_dim.65), calls=%async_computation.2 | async-start | bytes 573440 | tf_op jit(solution)/shard_map/all_to_all | solution.py:33
  108.4 0.6 fusion.15
  109.0 0.6 fusion
  109.6 1.5 copy.98
  111.1 9.3 %all-to-all-done.2 = f32[16,1,4480]{2,1,0:T(1,128)S(1)} async-done(((f32[16,1,4480]{2,1,0:T(1,128)}), f32[16,1,4480]{2,1,0:T(1,128)S(1)}, u32[]{:S(2)}, u32[]{:S(2)}) %all-to-all-start.2) | async-done | bytes 286752 | tf_op jit(solution)/shard_map/all_to_all | solution.py:33
  120.5 3.6 %all-to-all-start.1 = ((bf16[16,128,384]{1,2,0:T(8,128)(2,1)}), bf16[16,128,384]{1,2,0:T(8,128)(2,1)S(1)}, u32[]{:S(2)}, u32[]{:S(2)}) async-start(bf16[16,128,384]{1,2,0:T(8,128)(2,1)} %bitcast.72), calls=%async_computation.1 | async-start | bytes 3145728 | tf_op jit(solution)/shard_map/all_to_all | solution.py:57
  124.1 2.9 %multiply_reduce_fusion = (f32[192]{0:T(256)S(1)}, bf16[1,192,2048]{2,1,0:T(8,128)(2,1)}) fusion(bf16[768,2048]{1,0:T(8,128)(2,1)} %all-gather.2.cloned.1.call-done, f32[384]{0:T(512)S(1)} %reshape.153, f32[384,192]{0,1:T(8,128)S(1)} %fusion.13, f32[384,192]{0,1:T(8,128)S(1)} %fusion.11), kind=kOutput, calls=%fused_computation.2 | convolution fusion | flops 303685440 | bytes 2951424 | tf_op jit(solution)/shard_map/dot_general | solution.py:75
  127.0 0.2 reduce_sum.122
  127.2 0.2 convert_element_type.120
  127.5 34.4 %all-to-all-done.1 = bf16[16,128,384]{1,2,0:T(8,128)(2,1)S(1)} async-done(((bf16[16,128,384]{1,2,0:T(8,128)(2,1)}), bf16[16,128,384]{1,2,0:T(8,128)(2,1)S(1)}, u32[]{:S(2)}, u32[]{:S(2)}) %all-to-all-start.1) | async-done | bytes 1572896 | tf_op jit(solution)/shard_map/all_to_all | solution.py:57
  161.8 0.2 reduce_sum.118
  162.0 0.7 pad_maximum_fusion.2
  162.7 13.0 %all-to-all-start.3 = ((bf16[129,48,8]{0,2,1:T(8,128)(2,1)}), bf16[129,48,8]{0,2,1:T(8,128)(2,1)S(1)}, u32[]{:S(2)}, u32[]{:S(2)}) async-start(bf16[129,48,8]{0,2,1:T(8,128)(2,1)} %pad_maximum_fusion.2), calls=%async_computation.3 | async-start | bytes 393216 | tf_op jit(solution)/shard_map/all_to_all | solution.py:64
  175.7 0.6 broadcast_multiply_fusion
  176.3 0.6 slice_multiply_fusion
  176.9 13.5 %all-to-all-done.3 = bf16[129,48,8]{0,2,1:T(8,128)(2,1)S(1)} async-done(((bf16[129,48,8]{0,2,1:T(8,128)(2,1)}), bf16[129,48,8]{0,2,1:T(8,128)(2,1)S(1)}, u32[]{:S(2)}, u32[]{:S(2)}) %all-to-all-start.3) | async-done | bytes 99104 | tf_op jit(solution)/shard_map/all_to_all | solution.py:64
  190.4 0.1 convert_reduce_fusion
  190.5 0.1 reshape.154
  190.6 0.1 select_reduce_fusion
  190.7 0.1 reshape.150
  190.9 0.1 copy.90
  190.9 0.0 copy-done.6
  191.0 0.0 copy-done.4
  191.0 0.7 fusion.39
  191.8 5.5 %all-to-all-start.4 = ((f32[48,1,128]{2,1,0:T(1,128)}), f32[48,1,128]{2,1,0:T(1,128)S(1)}, u32[]{:S(2)}, u32[]{:S(2)}) async-start(f32[48,1,128]{2,1,0:T(1,128)} %bitcast.15), calls=%async_computation.4 | async-start | bytes 49152 | tf_op jit(solution)/shard_map/all_to_all | solution.py:70
  197.3 0.3 fusion.25
  197.5 1.5 convolution_add_fusion
  199.1 9.1 %all-to-all-done.4 = f32[48,1,128]{2,1,0:T(1,128)S(1)} async-done(((f32[48,1,128]{2,1,0:T(1,128)}), f32[48,1,128]{2,1,0:T(1,128)S(1)}, u32[]{:S(2)}, u32[]{:S(2)}) %all-to-all-start.4) | async-done | bytes 24608 | tf_op jit(solution)/shard_map/all_to_all | solution.py:70
  208.2 0.6 reduce_sum.126
  208.8 0.0 copy-done.5
  (19 shorter events, 0.2 us)
Async XLA Ops:
  7.2 89.1 %copy-start = (bf16[1,2048,192]{1,2,0:T(8,128)(2,1)S(1)}, bf16[1,2048,192]{1,2,0:T(8,128)(2,1)}, u32[]{:S(2)}) copy-start(bf16[1,2048,192]{1,2,0:T(8,128)(2,1)} %param.12) | copy-start | bytes 2359300
  7.2 89.1 %all-gather.2.cloned.1.call-start = ((), (), s32[]{:S(2)}) async-start(), calls=%async_computation.5 | async-start | bytes 3342336 | tf_op jit(solution)/shard_map/all_gather | solution.py:28
  49.8 48.8 %copy-start.2 = (bf16[1,2048,192]{1,2,0:T(8,128)(2,1)S(1)}, bf16[1,2048,192]{1,2,0:T(8,128)(2,1)}, u32[]{:S(2)}) copy-start(bf16[1,2048,192]{1,2,0:T(8,128)(2,1)} %param.13) | copy-start | bytes 2359300
  96.3 2.4 %copy-start.1 = (bf16[768,2048]{1,0:T(8,128)(2,1)S(1)}, bf16[768,2048]{1,0:T(8,128)(2,1)}, u32[]{:S(2)}) copy-start(bf16[768,2048]{1,0:T(8,128)(2,1)} %all-gather.2.cloned.1.call-done) | copy-start | bytes 9437188
  98.7 1.1 copy-start.7
  103.8 16.7 %all-to-all-start.2 = ((f32[16,1,4480]{2,1,0:T(1,128)}), f32[16,1,4480]{2,1,0:T(1,128)S(1)}, u32[]{:S(2)}, u32[]{:S(2)}) async-start(f32[16,1,4480]{2,1,0:T(1,128)} %broadcast_in_dim.65), calls=%async_computation.2 | async-start | bytes 573440 | tf_op jit(solution)/shard_map/all_to_all | solution.py:33
  120.5 41.3 %all-to-all-start.1 = ((bf16[16,128,384]{1,2,0:T(8,128)(2,1)}), bf16[16,128,384]{1,2,0:T(8,128)(2,1)S(1)}, u32[]{:S(2)}, u32[]{:S(2)}) async-start(bf16[16,128,384]{1,2,0:T(8,128)(2,1)} %bitcast.72), calls=%async_computation.1 | async-start | bytes 3145728 | tf_op jit(solution)/shard_map/all_to_all | solution.py:57
  127.0 63.9 %copy-start.6 = (bf16[128,2]{0,1:T(2,128)(2,1)S(1)}, bf16[128,2]{0,1:T(2,128)(2,1)}, u32[]{:S(2)}) copy-start(bf16[128,2]{0,1:T(2,128)(2,1)} %param.10) | copy-start | bytes 1540
  127.0 64.0 %copy-start.4 = (s32[128,2]{0,1:T(2,128)S(1)}, s32[128,2]{0,1:T(2,128)}, u32[]{:S(2)}) copy-start(s32[128,2]{0,1:T(2,128)} %param.9) | copy-start | bytes 3076
  127.0 64.0 %copy-start.3 = (bf16[128,128]{1,0:T(8,128)(2,1)S(1)}, bf16[128,128]{1,0:T(8,128)(2,1)}, u32[]{:S(2)}) copy-start(bf16[128,128]{1,0:T(8,128)(2,1)} %param.8) | copy-start | bytes 98308
  162.7 27.6 %all-to-all-start.3 = ((bf16[129,48,8]{0,2,1:T(8,128)(2,1)}), bf16[129,48,8]{0,2,1:T(8,128)(2,1)S(1)}, u32[]{:S(2)}, u32[]{:S(2)}) async-start(bf16[129,48,8]{0,2,1:T(8,128)(2,1)} %pad_maximum_fusion.2), calls=%async_computation.3 | async-start | bytes 393216 | tf_op jit(solution)/shard_map/all_to_all | solution.py:64
  190.9 17.8 %copy-start.5 = (f32[128,2]{0,1:T(2,128)}, f32[128,2]{0,1:T(2,128)S(1)}, u32[]{:S(2)}) copy-start(f32[128,2]{0,1:T(2,128)S(1)} %copy.90) | copy-start | bytes 3076
  191.8 16.4 %all-to-all-start.4 = ((f32[48,1,128]{2,1,0:T(1,128)}), f32[48,1,128]{2,1,0:T(1,128)S(1)}, u32[]{:S(2)}, u32[]{:S(2)}) async-start(f32[48,1,128]{2,1,0:T(1,128)} %bitcast.15), calls=%async_computation.4 | async-start | bytes 49152 | tf_op jit(solution)/shard_map/all_to_all | solution.py:70
Sparse Core Ops, SparseCore 0:
  50.6 45.6 all-gather.1
where the time goes:
time: 216 us
  waiting for transfers between devices  112 us (52%)
  blocking collectives  36.2 us (17%)
  starting transfers between devices  26.6 us (12%)
  matrix products  14.5 us (7%)
  between operations  14.3 us (7%)
  local copies, waits for them, and re-layouts  6.29 us (3%)
  other arithmetic  5.69 us (3%)
    all_gather x1, waiting for transfers between devices, sent_together(): lax.all_gather(both, axis, axis=dim, tiled=True)  45.6 us
    all_to_all x1, blocking collectives, side_by_side(): lax.all_to_all(both, axis, split_axis=split_dim, concat_axis=concat_dim,...  36.2 us
    all_to_all x1, waiting for transfers between devices, sum_at_owner(): lax.all_to_all(tiles, axis, split_axis=0, concat_axis=0, tiled=True)  34.4 us
    all_to_all x1, waiting for transfers between devices, sent_together_2(): lax.all_to_all(both, axis, split_axis=split_dim, concat_axis=concat_dim,...  13.5 us
    all_to_all x1, starting transfers between devices, sent_together_2(): lax.all_to_all(both, axis, split_axis=split_dim, concat_axis=concat_dim,...  13 us
    all_to_all x1, waiting for transfers between devices, sent_to_all(): return lax.all_to_all(copies, axis, split_axis=0, concat_axis=0, tiled=True)  9.35 us
    all_to_all x1, waiting for transfers between devices, sent_and_summed(): tiles = lax.all_to_all(cut_along(value, dim, peers), axis, 0, 0, tiled=True)  9.1 us
    dot_general x4, matrix products, matmul_tn(): lax.dot_general(left_side, right_side, (((0,), (0,)), ((), ())), preferre...  6.02 us
  transfers between devices with their start and end apart: 5, of which 5 were waited for; matrix products, arithmetic and copies ran while one was open for 4% of the time, Pallas kernels for 0%

commit v1 on v0

v1 whole, which is shorter than its diff:
```python
import functools

import jax
import jax.numpy as jnp
from jax import lax
from jax.experimental import pallas as pl
from jax.experimental.pallas import tpu as pltpu
from jax.sharding import PartitionSpec as P

MESH = pl.DeviceIdType.MESH
BF = jnp.bfloat16
F32 = jnp.float32
LANES = 128
HI = lax.Precision.HIGHEST


def dot(a, b, ca=1, cb=0, precision=None):
    return lax.dot_general(
        a, b, (((ca,), (cb,)), ((), ())), precision=precision, preferred_element_type=F32
    )


def log2(n):
    return n.bit_length() - 1


class Plan:
    def __init__(self, n_ep, n_tp, tok, width, hidden, features, cap):
        self.ep, self.tp, self.tok, self.width = n_ep, n_tp, tok, width
        self.hidden, self.features, self.cap = hidden, features, cap
        self.x = 4 if n_ep % 4 == 0 else 1
        self.z = n_ep // self.x
        self.y = n_tp // 2
        self.half = self.y // 2
        self.slots = n_ep * cap
        self.chunks = self.slots // LANES
        self.per_chunk = LANES // cap
        self.units = 4
        self.unit_rows = self.slots // self.units
        self.slab = 2 * width

    def near(self, dz):
        dz %= self.z
        if dz == 0:
            return 0
        return 2 * dz - 1 if 2 * dz <= self.z else 2 * (self.z - dz)

    def place(self, dz, dx):
        return self.near(dz) * self.x + dx % self.x

    def offsets(self):
        found = [(dz, dx) for dz in range(self.z) for dx in range(self.x) if (dz, dx) != (0, 0)]

        def hops(o):
            return min(o[0], self.z - o[0]) + min(o[1], self.x - o[1])

        return sorted(found, key=lambda o: (-hops(o), o[1], o[0]))

    def ring_units(self, k, way):
        low, high = 0, 2 * self.chunks
        if k == self.half:
            low, high = (0, self.chunks) if way == 0 else (self.chunks, 2 * self.chunks)
        out = []
        for u in range(self.chunks):
            a, b = max(low, 2 * u), min(high, 2 * u + 2)
            if a < b:
                out.append((u, a, b))
        return out

    def long_way(self, way, u):
        return (u < self.units // 2) == (way == 0)


def kernel(
    p,
    routing_ref, weight_ref, tokens_ref, cotangent_ref, gate_hbm, up_hbm, down_hbm, router_hbm,
    token_out, gate_out, dgate_hbm, dup_hbm, ddown_hbm, router_out, gsq_out, usq_out, dsq_out,
    w_gu, w_dn, r_cols, send_b, recv_b, w_send, w_recv, by_token, hits, places,
    g, pre, back, grads, grads_t, scaled, g_part, gp_recv, g_send, g_recv,
    mine, p_send, p_recv, rs_s, rs_r, c_buf, c_recv, rt_send, rt_recv, sq, sq_recv,
    dg, du, dd, d_acc,
    load_sem, disp_s, disp_r, wt_s, wt_r, ag_s, ag_r, pair_s, pair_r, gp_s, gp_r, gc_s, gc_r,
    ps_s, ps_r, rs_ss, rs_rs, cb_s, cb_r, rt_s, rt_r, sq_s, sq_r, out_sem,
):
    me = lax.axis_index("ep")
    t = lax.axis_index("tp")
    y, c = lax.div(t, 2), lax.rem(t, 2)
    z_me, x_me = lax.div(me, p.x), lax.rem(me, p.x)
    partner = t + 1 - 2 * c
    right = lax.rem(y + 1, p.y) * 2 + c
    left = lax.rem(y + p.y - 1, p.y) * 2 + c
    ways = (right, left)
    H, S, E, T, F = p.hidden, p.slots, p.ep, p.tok, p.width

    def peer(dz, dx):
        return lax.rem(z_me + dz, p.z) * p.x + lax.rem(x_me + dx, p.x)

    def remote(src, dst, s, r, to):
        return pltpu.make_async_remote_copy(
            src_ref=src, dst_ref=dst, send_sem=s, recv_sem=r, device_id=to, device_id_type=MESH
        )

    def wait_for(ref, sem):
        pltpu.make_async_copy(ref, ref, sem).wait()

    offsets = p.offsets()
    n_peers = len(offsets)
    loads = [
        pltpu.make_async_copy(gate_hbm, w_gu.at[pl.ds(0, H)], load_sem.at[0]),
        pltpu.make_async_copy(up_hbm, w_gu.at[pl.ds(H, H)], load_sem.at[1]),
        pltpu.make_async_copy(down_hbm, w_dn, load_sem.at[2]),
        pltpu.make_async_copy(
            router_hbm.at[:, pl.ds(pl.multiple_of(t * F, F), F)], r_cols, load_sem.at[3]
        ),
    ]
    barrier = pltpu.get_barrier_semaphore()
    for dz, dx in offsets:
        pl.semaphore_signal(barrier, inc=1, device_id=(peer(dz, dx), t), device_id_type=MESH)
    for j in range(1, p.tp):
        pl.semaphore_signal(
            barrier, inc=1, device_id=(me, lax.rem(t + j, p.tp)), device_id_type=MESH
        )
    for copy in loads:
        copy.start()

    routes = routing_ref[...]
    expert_rows = lax.broadcasted_iota(jnp.int32, (E, T), 0)
    hit = [(expert_rows == routes[k : k + 1, :]).astype(F32) for k in range(2)]
    earlier = (
        lax.broadcasted_iota(jnp.int32, (T, T), 0) < lax.broadcasted_iota(jnp.int32, (T, T), 1)
    ).astype(F32).astype(BF)
    count = dot((hit[0] + hit[1]).astype(BF), earlier)
    pos = [jnp.sum(hit[k] * count, axis=0, keepdims=True) for k in range(2)]
    slot_rows = lax.broadcasted_iota(jnp.int32, (S, T), 0).astype(F32)
    slot = [routes[k : k + 1, :].astype(F32) * p.cap + pos[k] for k in range(2)]
    match = jnp.where((slot_rows == slot[0]) | (slot_rows == slot[1]), 1.0, 0.0)
    tokens = tokens_ref[...]
    match_b = match.astype(BF)
    in_rows = dot(match_b, tokens).reshape(E, p.cap, F)
    tan_rows = dot(match_b, cotangent_ref[...]).reshape(E, p.cap, F)
    send_b[...] = jnp.concatenate([in_rows, tan_rows], axis=1).astype(BF)
    for k in range(2):
        hits[k] = hit[k]
        places[k] = pos[k]
    weights = weight_ref[...].astype(F32)
    lane_rows = lax.broadcasted_iota(jnp.int32, (LANES, T), 0)
    lane_slot = (lane_rows & (p.cap - 1)).astype(F32)
    spread = sum(
        dot(hit[k].astype(BF), jnp.where(lane_slot == pos[k], weights[k : k + 1, :], 0.0).astype(BF), 1, 1)
        for k in range(2)
    )
    e_ids = lax.broadcasted_iota(jnp.int32, (E, LANES), 0)
    lane_ids = lax.broadcasted_iota(jnp.int32, (E, LANES), 1)
    dz = z_me - (e_ids >> log2(p.x))
    dz = jnp.where(dz < 0, dz + p.z, dz)
    near = jnp.where(dz == 0, 0, jnp.where(2 * dz <= p.z, 2 * dz - 1, 2 * (p.z - dz)))
    my_place = near * p.x + ((x_me - (e_ids & (p.x - 1))) & (p.x - 1))
    my_lanes = (lane_ids >> log2(p.cap)) == (my_place & (p.per_chunk - 1))
    w_send[...] = jnp.where(my_lanes, spread, 0.0).reshape(E, 1, LANES)

    pl.semaphore_wait(barrier, n_peers + p.tp - 1)

    for dz, dx in offsets:
        to = peer(dz, dx)
        at = p.place(-dz, -dx)
        remote(send_b.at[to], recv_b.at[at], disp_s, disp_r.at[at // p.per_chunk], (to, t)).start()
        remote(w_send.at[to], w_recv.at[at], wt_s, wt_r, (to, t)).start()
    recv_b[0] = send_b[me]
    w_recv[0] = w_send[me]
    by_token[...] = match.T.astype(BF)

    sent = []

    def move(k, way, u, a, b):
        r = (-(k - 1) if way == 0 else k - 1) % p.y
        to_r = (-k if way == 0 else k) % p.y
        copy = remote(
            g.at[r, c, pl.ds(a, b - a)], g.at[to_r, c, pl.ds(a, b - a)],
            ag_s.at[way, k - 1, u], ag_r.at[way, k - 1, u], (me, ways[way]),
        )
        copy.start()
        sent.append(copy)

    def to_partner(r, u, a, b, s):
        piece = g.at[r, c, pl.ds(a, b - a)]
        copy = remote(piece, piece, pair_s.at[r, s], pair_r.at[r, s], (me, partner))
        copy.start()
        sent.append(copy)

    def pair_pieces(r):
        if r == p.half:
            found = [w for way in range(2) for w in p.ring_units(p.half, way)]
        else:
            found = p.ring_units(1 if p.half > 1 else 0, 0)
        return [(s, a, b) for s, (_, a, b) in enumerate(found)]

    def from_partner(r):
        for s, a, b in pair_pieces(r):
            wait_for(g.at[r, 1 - c, pl.ds(a, b - a)], pair_r.at[r, s])

    def semaphore_of(r, a):
        return [s for s, first, _ in pair_pieces(r) if first == a][0]

    def lanes_of(r):
        return pl.ds(pl.multiple_of(lax.rem(y + r, p.y) * p.slab, p.slab), p.slab)

    def rows_of(r, kind):
        return jnp.concatenate(
            [
                jnp.concatenate([g[r, core, 2 * ch + kind] for ch in range(p.chunks)], axis=0)
                for core in range(2)
            ],
            axis=1,
        )

    def forward(r, first):
        from_partner(r)
        cols = lanes_of(r)
        up = dot(w_gu[:, cols], rows_of(r, 0), 1, 1)
        down = dot(w_dn[:, cols], rows_of(r, 1), 1, 1)
        if first:
            pre[...] = up
            back[...] = down
        else:
            pre[...] += up
            back[...] += down

    for u in range(p.chunks):
        arrived = p.per_chunk - (1 if u == 0 else 0)
        if arrived:
            wait_for(recv_b.at[pl.ds(0, arrived)], disp_r.at[u])
        both = recv_b[u * p.per_chunk : (u + 1) * p.per_chunk].astype(F32)
        g[0, c, 2 * u] = both[:, : p.cap].reshape(LANES, F).astype(BF)
        g[0, c, 2 * u + 1] = both[:, p.cap :].reshape(LANES, F).astype(BF)
        for way in range(2):
            for v, a, b in p.ring_units(1, way):
                if v == u:
                    move(1, way, v, a, b)
        to_partner(0, u, 2 * u, 2 * u + 2, u)
    for copy in loads:
        copy.wait()
    wait_for(w_recv.at[pl.ds(0, n_peers)], wt_r)
    slot_weight = jnp.concatenate(
        [
            jnp.sum(w_recv[ch * p.per_chunk : (ch + 1) * p.per_chunk], axis=0)
            for ch in range(p.chunks)
        ],
        axis=1,
    )
    for k in range(1, p.half + 1):
        if k == p.half:
            for r in sorted({(k - 1) % p.y, (1 - k) % p.y}):
                forward(r, r == 0)
        for u in range(p.chunks):
            for way in range(2):
                r = (-k if way == 0 else k) % p.y
                for v, a, b in p.ring_units(k, way):
                    if v != u:
                        continue
                    wait_for(g.at[r, c, pl.ds(a, b - a)], ag_r.at[way, k - 1, v])
                    if k < p.half:
                        for v2, a2, b2 in p.ring_units(k + 1, way):
                            if v2 == u:
                                move(k + 1, way, v2, a2, b2)
                    to_partner(r, u, a, b, semaphore_of(r, a))
        if k < p.half:
            for r in sorted({(k - 1) % p.y, (1 - k) % p.y}):
                forward(r, r == 0)
    forward(p.half, False)

    part = jnp.zeros((1, S), F32)
    step = 32
    for b in range(0, H, step):
        pg, pu, bp = pre[b : b + step, :], pre[H + b : H + b + step, :], back[b : b + step, :]
        sig = lax.logistic(pg)
        act = pg * sig
        hid = act * pu
        part = part + jnp.sum(hid * bp, axis=0, keepdims=True)
        scaled[b : b + step, :] = (slot_weight * hid).astype(BF)
        hg = slot_weight * bp
        grads[b : b + step, :] = (hg * pu * sig * (1.0 + pg * (1.0 - sig))).astype(BF)
        grads[H + b : H + b + step, :] = (hg * act).astype(BF)
    for ch in range(p.chunks):
        g_part[ch : ch + 1, :] = part[:, ch * LANES : (ch + 1) * LANES]
    g_part[p.chunks :, :] = jnp.zeros((8 - p.chunks, LANES), F32)
    gp_recv[t] = g_part[...]
    for j in range(1, p.tp):
        remote(g_part, gp_recv.at[t], gp_s, gp_r, (me, lax.rem(t + j, p.tp))).start()
    grads_t[...] = grads[...].astype(F32).T.astype(BF)

    def slot_block(r):
        block = dot(grads_t[...], w_gu[:, lanes_of(r)])
        low, high = block[:, :F], block[:, F:]
        mine[r] = jnp.where(c == 0, low, high).astype(BF)
        p_send[r] = jnp.where(c == 0, high, low).astype(BF)
        copy = remote(p_send.at[r], p_recv.at[r], ps_s.at[r], ps_r.at[r], (me, partner))
        copy.start()
        sent.append(copy)

    def chip_sum(r, u):
        rows = pl.ds(u * p.unit_rows, p.unit_rows)
        return mine[r, rows].astype(F32) + p_recv[r, rows].astype(F32)

    def ring_send(way, u, d):
        r = (d if way == 0 else -d) % p.y
        total = chip_sum(r, u)
        longest = p.half if p.long_way(way, u) else p.half - 1
        if d < longest:
            wait_for(rs_r.at[way, u, d], rs_rs.at[way, u, d])
            total = total + rs_r[way, u, d].astype(F32)
        rs_s[way, u, d - 1] = total.astype(BF)
        copy = remote(
            rs_s.at[way, u, d - 1], rs_r.at[way, u, d - 1],
            rs_ss.at[way, u, d - 1], rs_rs.at[way, u, d - 1], (me, ways[way]),
        )
        copy.start()
        sent.append(copy)

    def ring_step(j):
        for u in range(p.units // 2):
            for way in range(2):
                v = u if way == 0 else u + p.units // 2
                if p.half - j + 1 >= 1:
                    ring_send(way, v, p.half - j + 1)
        for u in range(p.units // 2):
            for way in range(2):
                v = u + p.units // 2 if way == 0 else u
                if p.half - j >= 1:
                    ring_send(way, v, p.half - j)

    order = [p.half]
    for d in range(p.half - 1, 0, -1):
        order += [d, p.y - d]
    order.append(0)
    first = 1 if p.half == 1 else 3
    for r in order[:first]:
        slot_block(r)
    for r in order[:first]:
        wait_for(p_recv.at[r], ps_r.at[r])
    ring_step(1)
    for r in order[first:]:
        slot_block(r)
    for r in order[first:]:
        wait_for(p_recv.at[r], ps_r.at[r])

    d_acc[...] = jnp.zeros_like(d_acc)

    def weight_grads(r):
        cols = lanes_of(r)
        both = dot(grads[...], rows_of(r, 0))
        dg[:, cols] = both[:H].astype(BF)
        du[:, cols] = both[H:].astype(BF)
        sq[0:1, cols] = jnp.sum(both[:H] * both[:H], axis=0, keepdims=True)
        sq[1:2, cols] = jnp.sum(both[H:] * both[H:], axis=0, keepdims=True)
        down = dot(scaled[...], rows_of(r, 1))
        dd[:, cols] = down.astype(BF)
        square = down * down
        d_acc[...] += square[:, :F] + square[:, F:]

    slabs = list(range(p.y))
    per_step = -(-p.y // max(1, p.half - 1)) if p.half > 1 else p.y
    gate_done = False

    def gate_sum():
        wait_for(gp_recv.at[pl.ds(0, p.tp - 1)], gp_r)
        total = jnp.sum(gp_recv[...], axis=0)
        for ch in range(p.chunks):
            g_send[ch] = total[ch : ch + 1, :]
        for dz, dx in offsets:
            to = peer(dz, dx)
            row = p.place(dz, dx) // p.per_chunk
            remote(g_send.at[row], g_recv.at[me], gc_s, gc_r, (to, t)).start()
        g_recv[me] = g_send[0]

    for j in range(2, p.half + 1):
        for r in slabs[:per_step]:
            weight_grads(r)
        slabs = slabs[per_step:]
        ring_step(j)
        if not gate_done:
            gate_sum()
            gate_done = True
    for r in slabs:
        weight_grads(r)
    if not gate_done:
        gate_sum()
    outs = [
        pltpu.make_async_copy(dg, dgate_hbm, out_sem.at[0]),
        pltpu.make_async_copy(du, dup_hbm, out_sem.at[1]),
        pltpu.make_async_copy(dd, ddown_hbm, out_sem.at[2]),
    ]
    for copy in outs:
        copy.start()

    totals = []
    for u in range(p.units):
        total = chip_sum(0, u)
        for way in range(2):
            if p.half > 1 or p.long_way(way, u):
                wait_for(rs_r.at[way, u, 0], rs_rs.at[way, u, 0])
                total = total + rs_r[way, u, 0].astype(F32)
        totals.append(total)
    c_buf[...] = jnp.concatenate(totals, axis=0).reshape(E, p.cap, F).astype(BF)

    for dz, dx in offsets:
        to = peer(dz, dx)
        remote(c_buf.at[p.place(dz, dx)], c_recv.at[me], cb_s, cb_r, (to, t)).start()
    c_recv[me] = c_buf[0]

    wait_for(g_recv.at[pl.ds(0, n_peers)], gc_r)
    kept = jnp.where(my_lanes, g_recv[...].reshape(E, LANES), 0.0)
    gate = []
    for k in range(2):
        picked = dot(kept, hits[k], 0, 0, HI)
        gate.append(jnp.sum(jnp.where(lane_slot == places[k], picked, 0.0), axis=0, keepdims=True))
        gate_out[k : k + 1, :] = gate[k]
    mixed = weights[0:1, :] * gate[0] + weights[1:2, :] * gate[1]
    logit = [weights[k : k + 1, :] * (gate[k] - mixed) for k in range(2)]
    signal = (hits[0] * logit[0] + hits[1] * logit[1]).astype(BF)
    rt_send[...] = dot(signal, tokens).reshape(E, 1, F)
    for dz, dx in offsets:
        to = peer(dz, dx)
        remote(rt_send.at[to], rt_recv.at[me], rt_s, rt_r, (to, t)).start()
    rt_recv[me] = rt_send[me]
    sq_recv[t] = sq[...]
    for j in range(1, p.tp):
        remote(sq, sq_recv.at[t], sq_s, sq_r, (me, lax.rem(t + j, p.tp))).start()
    from_router = dot(signal.astype(F32).T.astype(BF), r_cols[...])
    ones = jnp.ones((8, F), F32)
    dsq_out[...] = dot(ones, d_acc[...], 1, 1, HI)[0:1, :] * (1.0 / p.features)

    wait_for(c_recv.at[pl.ds(0, n_peers)], cb_r)
    rows = c_recv[...].astype(F32).reshape(S, F).astype(BF)
    token_out[...] = dot(by_token[...], rows) + from_router
    wait_for(rt_recv.at[pl.ds(0, n_peers)], rt_r)
    router_out[...] = jnp.sum(rt_recv[...], axis=0)
    wait_for(sq_recv.at[pl.ds(0, p.tp - 1)], sq_r)
    squares = jnp.sum(sq_recv[...], axis=0) * (1.0 / (H * p.tp))
    gsq_out[...] = squares[0:1, :]
    usq_out[...] = squares[1:2, :]

    for copy in sent:
        copy.wait_send()
    wait_for(send_b.at[pl.ds(0, n_peers)], disp_s)
    wait_for(w_send.at[pl.ds(0, n_peers)], wt_s)
    wait_for(gp_recv.at[pl.ds(0, p.tp - 1)], gp_s)
    wait_for(g_recv.at[pl.ds(0, n_peers)], gc_s)
    wait_for(c_recv.at[pl.ds(0, n_peers)], cb_s)
    wait_for(rt_recv.at[pl.ds(0, n_peers)], rt_s)
    wait_for(sq_recv.at[pl.ds(0, p.tp - 1)], sq_s)
    for copy in outs:
        copy.wait()


def run(p, routing, weights, tokens, cotangent, gate_t, up_t, down, router_t):
    H, S, E, T, F, D, N = p.hidden, p.slots, p.ep, p.tok, p.width, p.features, p.tp
    vm, hbm = pl.BlockSpec(memory_space=pltpu.VMEM), pl.BlockSpec(memory_space=pl.ANY)
    V, dma = pltpu.VMEM, pltpu.SemaphoreType.DMA
    scratch = [
        V((2 * H, D), BF), V((H, D), BF), V((E, F), BF),
        V((E, 2 * p.cap, F), BF), V((E, 2 * p.cap, F), BF),
        V((E, 1, LANES), F32), V((E, 1, LANES), F32),
        V((T, S), BF), V((2, E, T), F32), V((2, 1, T), F32),
        V((p.y, 2, 2 * p.chunks, LANES, F), BF),
        V((2 * H, S), F32), V((H, S), F32), V((2 * H, S), BF), V((S, 2 * H), BF), V((H, S), BF),
        V((8, LANES), F32), V((N, 8, LANES), F32), V((p.chunks, 1, LANES), F32), V((E, 1, LANES), F32),
        V((p.y, S, F), BF), V((p.y, S, F), BF), V((p.y, S, F), BF),
        V((2, p.units, p.half, p.unit_rows, F), BF), V((2, p.units, p.half, p.unit_rows, F), BF),
        V((E, p.cap, F), BF), V((E, p.cap, F), BF),
        V((E, 1, F), F32), V((E, 1, F), F32),
        V((2, D), F32), V((N, 2, D), F32),
        V((H, D), BF), V((H, D), BF), V((H, D), BF), V((H, F), F32),
        dma((4,)), dma, dma((p.chunks,)), dma, dma,
        dma((2, p.half, p.chunks)), dma((2, p.half, p.chunks)),
        dma((p.y, p.chunks + 1)), dma((p.y, p.chunks + 1)),
        dma, dma, dma, dma,
        dma((p.y,)), dma((p.y,)),
        dma((2, p.units, p.half)), dma((2, p.units, p.half)),
        dma, dma, dma, dma, dma, dma, dma((3,)),
    ]
    shape = jax.ShapeDtypeStruct
    return pl.pallas_call(
        functools.partial(kernel, p),
        out_shape=(
            shape((T, F), F32), shape((2, T), F32),
            shape((H, D), BF), shape((H, D), BF), shape((H, D), BF),
            shape((1, F), F32), shape((1, D), F32), shape((1, D), F32), shape((1, H), F32),
        ),
        in_specs=[vm, vm, vm, vm, hbm, hbm, hbm, hbm],
        out_specs=(vm, vm, hbm, hbm, hbm, vm, vm, vm, vm),
        scratch_shapes=scratch,
        compiler_params=pltpu.CompilerParams(
            collective_id=0, has_side_effects=True, vmem_limit_bytes=48 << 20
        ),
        name="expert_backward",
    )(routing, weights, tokens, cotangent, gate_t, up_t, down, router_t)


def shards(tokens, routing, gate_weights, cotangent, expert_gate, expert_up, expert_down, router):
    tok, width = tokens.shape
    n_ep, n_tp = lax.axis_size("ep"), lax.axis_size("tp")
    experts = router.shape[1]
    cap = 3 * routing.shape[1] * tok // (2 * experts)
    p = Plan(n_ep, n_tp, tok, width, expert_gate.shape[2], width * n_tp, cap)
    out = run(
        p, routing.T, gate_weights.T, tokens, cotangent,
        expert_gate[0].T, expert_up[0].T, expert_down[0], router.T,
    )
    token_grad, gate_grad, dgate, dup, ddown, router_grad, gsq, usq, dsq = out
    return (
        token_grad, gate_grad.T, dgate.T[None], dup.T[None], ddown[None], router_grad, gsq, usq, dsq,
    )


def solution(mesh):
    in_specs = (
        P("ep", "tp"),
        P("ep", None),
        P("ep", None),
        P("ep", "tp"),
        P("ep", None, "tp"),
        P("ep", None, "tp"),
        P("ep", "tp", None),
        P(),
    )
    out_specs = (
        P("ep", "tp"),
        P("ep", None),
        P("ep", None, "tp"),
        P("ep", None, "tp"),
        P("ep", "tp", None),
        P("ep", "tp"),
        P("ep", None),
        P("ep", None),
        P("ep", "tp"),
    )
    return jax.shard_map(shards, mesh=mesh, in_specs=in_specs, out_specs=out_specs, check_vma=False)
```

time: 216 us -> 91.4 us (0.42)
  waiting for transfers between devices: 112 us -> 0 us
  Pallas kernels: 0 us -> 77.6 us
  blocking collectives: 36.2 us -> 0 us
  starting transfers between devices: 26.6 us -> 0 us
  matrix products: 14.5 us -> 0 us
  between operations: 14.3 us -> 0.68 us
  local copies, waits for them, and re-layouts: 6.29 us -> 12.6 us
  other arithmetic: 5.69 us -> 0 us
    pallas_call x0 -> x1, Pallas kernels: none -> 77.6 us  [run(): pl.pallas_call(functools.partial(kernel, p), out_shape=(shape((T, F), F32...]
    all_to_all x4 -> x0, waiting for transfers between devices: 66.3 us -> none  [the longest x1 34.4 us: sum_at_owner(): lax.all_to_all(tiles, axis, split_axis=0, concat_axis=0, tiled=True)]
    all_gather x1 -> x0, waiting for transfers between devices: 45.6 us -> none  [sent_together(): lax.all_gather(both, axis, axis=dim, tiled=True)]
    all_to_all x1 -> x0, blocking collectives: 36.2 us -> none  [side_by_side(): lax.all_to_all(both, axis, split_axis=split_dim, concat_axis=concat_dim,...]
    all_to_all x4 -> x0, starting transfers between devices: 26.6 us -> none  [the longest x1 13 us: sent_together_2(): lax.all_to_all(both, axis, split_axis=split_dim, concat_axis=concat_dim,...]
    dot_general x13 -> x0, matrix products: 14.5 us -> none  [the longest x4 6.02 us: matmul_tn(): lax.dot_general(left_side, right_side, (((0,), (0,)), ((), ())), preferre...]
    unnamed x17 -> x25, local copies, waits for them, and re-layouts: 1.44 us -> 12.6 us
  transfers between devices with their start and end apart: 5 -> 0, of which waited for: 5 -> 0; matrix products, arithmetic and copies ran while one was open for 4% -> 0% of each run, Pallas kernels for 0% -> 0%
where the time goes in v1:
time: 91.4 us; the launch traced here: 90.9 us
  Pallas kernels  77.6 us (85%)
  local copies, waits for them, and re-layouts  12.6 us (14%)
    pallas_call x1, Pallas kernels, run(): pl.pallas_call(functools.partial(kernel, p), out_shape=(shape((T, F), F32...  77.6 us
    unnamed x25, local copies, waits for them, and re-layouts  12.6 us

profile of v1, /device:TPU:1, one launch (start us, length us, event | category | flops | bytes accessed | tf_op | source)
XLA Modules:
  0.0 90.9 jit_solution(7331850898201040255)
XLA Ops:
  0.6 0.0 copy-start.6
  0.7 0.0 copy-start.7
  0.7 0.7 copy-done.6
  1.3 0.0 copy-done.7
  1.3 0.0 copy-start
  1.3 1.1 %copy-done = bf16[1,2048,192]{1,2,0:T(8,128)(2,1)S(1)} copy-done((bf16[1,2048,192]{1,2,0:T(8,128)(2,1)S(1)}, bf16[1,2048,192]{1,2,0:T(8,128)(2,1)}, u32[]{:S(2)}) %copy-start) | copy-done | bytes 786456
  2.5 0.0 copy-start.1
  2.5 1.1 %copy-done.1 = bf16[1,2048,192]{1,2,0:T(8,128)(2,1)S(1)} copy-done((bf16[1,2048,192]{1,2,0:T(8,128)(2,1)S(1)}, bf16[1,2048,192]{1,2,0:T(8,128)(2,1)}, u32[]{:S(2)}) %copy-start.1) | copy-done | bytes 786456
  3.6 0.0 copy-start.2
  3.6 1.1 %copy-done.2 = bf16[1,192,2048]{2,1,0:T(8,128)(2,1)S(1)} copy-done((bf16[1,192,2048]{2,1,0:T(8,128)(2,1)S(1)}, bf16[1,192,2048]{2,1,0:T(8,128)(2,1)}, u32[]{:S(2)}) %copy-start.2) | copy-done | bytes 786456
  4.7 0.0 copy-start.3
  4.7 0.9 %copy-done.3 = bf16[2048,48]{0,1:T(8,128)(2,1)S(1)} copy-done((bf16[2048,48]{0,1:T(8,128)(2,1)S(1)}, bf16[2048,48]{0,1:T(8,128)(2,1)}, u32[]{:S(2)}) %copy-start.3) | copy-done | bytes 196632
  5.7 0.0 copy-start.4
  5.7 0.8 copy-done.4
  6.4 0.0 copy-start.5
  6.4 0.8 copy-done.5
  7.2 77.6 %expert_backward.1 = (f32[128,128]{1,0:T(8,128)S(1)}, f32[2,128]{1,0:T(2,128)S(1)}, bf16[192,2048]{1,0:T(8,128)(2,1)S(1)}, bf16[192,2048]{1,0:T(8,128)(2,1)S(1)}...) custom-call(s32[2,128]{1,0:T(2,128)S(1)} %bitcast.25, ...), custom_call_target="tpu_custom_call" | custom-call | tf_op jit(solution)/shard_map/expert_backward/pallas_call | solution.py:482
  84.8 0.6 copy.26
  85.5 0.6 copy.27
  86.0 0.9 copy.28
  86.9 0.9 copy.29
  87.8 0.9 copy.30
  88.7 0.5 copy.31
  89.2 0.6 copy.32
  89.8 0.6 copy.33
  90.4 0.6 copy.34
Async XLA Ops:
  0.6 0.7 copy-start.6
  0.7 0.7 copy-start.7
  1.3 1.1 %copy-start = (bf16[1,2048,192]{1,2,0:T(8,128)(2,1)S(1)}, bf16[1,2048,192]{1,2,0:T(8,128)(2,1)}, u32[]{:S(2)}) copy-start(bf16[1,2048,192]{1,2,0:T(8,128)(2,1)} %param.12) | copy-start | bytes 2359300
  2.5 1.1 %copy-start.1 = (bf16[1,2048,192]{1,2,0:T(8,128)(2,1)S(1)}, bf16[1,2048,192]{1,2,0:T(8,128)(2,1)}, u32[]{:S(2)}) copy-start(bf16[1,2048,192]{1,2,0:T(8,128)(2,1)} %param.13) | copy-start | bytes 2359300
  3.6 1.1 %copy-start.2 = (bf16[1,192,2048]{2,1,0:T(8,128)(2,1)S(1)}, bf16[1,192,2048]{2,1,0:T(8,128)(2,1)}, u32[]{:S(2)}) copy-start(bf16[1,192,2048]{2,1,0:T(8,128)(2,1)} %param.14) | copy-start | bytes 2359300
  4.7 0.9 %copy-start.3 = (bf16[2048,48]{0,1:T(8,128)(2,1)S(1)}, bf16[2048,48]{0,1:T(8,128)(2,1)}, u32[]{:S(2)}) copy-start(bf16[2048,48]{0,1:T(8,128)(2,1)} %param.15) | copy-start | bytes 589828
  5.7 0.8 copy-start.4
  6.4 0.8 copy-start.5

commit v2 on v1

v2 whole, which is shorter than its diff:
```python
import functools

import jax
import jax.numpy as jnp
from jax import lax
from jax.experimental import pallas as pl
from jax.experimental.pallas import tpu as pltpu
from jax.sharding import PartitionSpec as P

MESH = pl.DeviceIdType.MESH
BF = jnp.bfloat16
F32 = jnp.float32
LANES = 128
HI = lax.Precision.HIGHEST


def dot(a, b, ca=1, cb=0, precision=None):
    return lax.dot_general(
        a, b, (((ca,), (cb,)), ((), ())), precision=precision, preferred_element_type=F32
    )


def log2(n):
    return n.bit_length() - 1


class Marks:
    def __init__(self):
        self.scope = None

    def __call__(self, name):
        if self.scope is not None:
            self.scope.__exit__(None, None, None)
        self.scope = jax.named_scope(name) if name else None
        if name:
            self.scope.__enter__()


class Plan:
    def __init__(self, n_ep, n_tp, tok, width, hidden, features, cap):
        self.ep, self.tp, self.tok, self.width = n_ep, n_tp, tok, width
        self.hidden, self.features, self.cap = hidden, features, cap
        self.x = 4 if n_ep % 4 == 0 else 1
        self.z = n_ep // self.x
        self.y = n_tp // 2
        self.half = self.y // 2
        self.slots = n_ep * cap
        self.chunks = self.slots // LANES
        self.per_chunk = LANES // cap
        self.units = 4
        self.unit_rows = self.slots // self.units
        self.slab = 2 * width

    def near(self, dz):
        dz %= self.z
        if dz == 0:
            return 0
        return 2 * dz - 1 if 2 * dz <= self.z else 2 * (self.z - dz)

    def place(self, dz, dx):
        return self.near(dz) * self.x + dx % self.x

    def offsets(self):
        found = [(dz, dx) for dz in range(self.z) for dx in range(self.x) if (dz, dx) != (0, 0)]

        def hops(o):
            return min(o[0], self.z - o[0]) + min(o[1], self.x - o[1])

        return sorted(found, key=lambda o: (-hops(o), o[1], o[0]))

    def ring_units(self, k, way):
        kinds = (way,) if k == self.half else (0, 1)
        return [(u, 2 * u + kind) for u in range(self.chunks) for kind in kinds]

    def early(self):
        return sorted(self.offsets(), key=lambda o: self.place(-o[0], -o[1]) // self.per_chunk)

    def gather_order(self):
        if self.half == 4 and self.chunks == 3:
            a, p, m = "arrive", "pass", "multiply"
            return (
                (a, 0, 0), (a, 0, 1), (p, 1, 0), (a, 0, 2), (p, 1, 1), (p, 2, 0), (p, 1, 2),
                (p, 2, 1), (m, 0, 0), (p, 3, 0), (p, 2, 2), (p, 3, 1), (m, 1, 0), (p, 4, 0),
                (p, 3, 2), (m, 2, 0), (p, 4, 1), (p, 4, 2), (m, 3, 0), (m, 4, 0),
            )
        out = [("arrive", 0, u) for u in range(self.chunks)] + [("multiply", 0, 0)]
        for k in range(1, self.half + 1):
            out += [("pass", k, u) for u in range(self.chunks)] + [("multiply", k, 0)]
        return out

    def long_way(self, way, u):
        return u % 2 == way


def kernel(
    p,
    routing_hbm, weight_hbm, tokens_hbm, cotangent_hbm, gate_hbm, up_hbm, down_hbm, router_hbm,
    token_out, gate_out, dg, du, dd, router_out, gsq_out, usq_out, dsq_out,
    routing_ref, weight_ref, tokens_ref, cotangent_ref,
    w_gu, w_dn, r_cols, send_b, recv_b, w_send, w_recv, by_token, hits, places,
    g, pre, back, grads, grads_t, scaled, g_part, gp_recv, g_send, g_recv,
    mine, p_send, p_recv, rs_s, rs_r, c_buf, c_recv, rt_send, rt_recv, sq, sq_recv, sq_sum, sq_all,
    d_acc,
    load_sem, disp_s, disp_r, wt_s, wt_r, ag_s, ag_r, pair_s, pair_r, gp_s, gp_r, gc_s, gc_r,
    ps_s, ps_r, rs_ss, rs_rs, cb_s, cb_r, rt_s, rt_r, sq_s, sq_r, sa_s, sa_r,
):
    mark = Marks()
    mark("start")
    me = lax.axis_index("ep")
    t = lax.axis_index("tp")
    y, c = lax.div(t, 2), lax.rem(t, 2)
    z_me, x_me = lax.div(me, p.x), lax.rem(me, p.x)
    partner = t + 1 - 2 * c
    right = lax.rem(y + 1, p.y) * 2 + c
    left = lax.rem(y + p.y - 1, p.y) * 2 + c
    ways = (right, left)
    H, S, E, T, F = p.hidden, p.slots, p.ep, p.tok, p.width

    def peer(dz, dx):
        return lax.rem(z_me + dz, p.z) * p.x + lax.rem(x_me + dx, p.x)

    def remote(src, dst, s, r, to):
        return pltpu.make_async_remote_copy(
            src_ref=src, dst_ref=dst, send_sem=s, recv_sem=r, device_id=to, device_id_type=MESH
        )

    def wait_for(ref, sem):
        pltpu.make_async_copy(ref, ref, sem).wait()

    offsets = p.offsets()
    n_peers = len(offsets)
    first_loads = [
        pltpu.make_async_copy(routing_hbm, routing_ref, load_sem.at[4]),
        pltpu.make_async_copy(weight_hbm, weight_ref, load_sem.at[5]),
        pltpu.make_async_copy(tokens_hbm, tokens_ref, load_sem.at[6]),
        pltpu.make_async_copy(cotangent_hbm, cotangent_ref, load_sem.at[7]),
    ]
    loads = [
        pltpu.make_async_copy(gate_hbm, w_gu.at[pl.ds(0, H)], load_sem.at[0]),
        pltpu.make_async_copy(up_hbm, w_gu.at[pl.ds(H, H)], load_sem.at[1]),
        pltpu.make_async_copy(down_hbm, w_dn, load_sem.at[2]),
        pltpu.make_async_copy(
            router_hbm.at[:, pl.ds(pl.multiple_of(t * F, F), F)], r_cols, load_sem.at[3]
        ),
    ]
    for copy in first_loads:
        copy.start()
    barrier = pltpu.get_barrier_semaphore()
    for dz, dx in offsets:
        pl.semaphore_signal(barrier, inc=1, device_id=(peer(dz, dx), t), device_id_type=MESH)
    for j in range(1, p.tp):
        pl.semaphore_signal(
            barrier, inc=1, device_id=(me, lax.rem(t + j, p.tp)), device_id_type=MESH
        )
    for copy in loads:
        copy.start()

    for copy in first_loads:
        copy.wait()
    mark("tables")

    routes = routing_ref[...]
    expert_rows = lax.broadcasted_iota(jnp.int32, (E, T), 0)
    hit = [(expert_rows == routes[k : k + 1, :]).astype(F32) for k in range(2)]
    earlier = (
        lax.broadcasted_iota(jnp.int32, (T, T), 0) < lax.broadcasted_iota(jnp.int32, (T, T), 1)
    ).astype(F32).astype(BF)
    count = dot((hit[0] + hit[1]).astype(BF), earlier)
    pos = [jnp.sum(hit[k] * count, axis=0, keepdims=True) for k in range(2)]
    slot_rows = lax.broadcasted_iota(jnp.int32, (S, T), 0).astype(F32)
    slot = [routes[k : k + 1, :].astype(F32) * p.cap + pos[k] for k in range(2)]
    match = jnp.where((slot_rows == slot[0]) | (slot_rows == slot[1]), 1.0, 0.0)
    tokens = tokens_ref[...]
    match_b = match.astype(BF)
    in_rows = dot(match_b, tokens).reshape(E, p.cap, F)
    tan_rows = dot(match_b, cotangent_ref[...]).reshape(E, p.cap, F)
    send_b[...] = jnp.concatenate([in_rows, tan_rows], axis=1).astype(BF)
    for k in range(2):
        hits[:, k * T : (k + 1) * T] = hit[k]
        places[:, k * T : (k + 1) * T] = pos[k]
    weights = weight_ref[...].astype(F32)
    lane_rows = lax.broadcasted_iota(jnp.int32, (LANES, T), 0)
    lane_slot = (lane_rows & (p.cap - 1)).astype(F32)
    spread = sum(
        dot(hit[k].astype(BF), jnp.where(lane_slot == pos[k], weights[k : k + 1, :], 0.0).astype(BF), 1, 1)
        for k in range(2)
    )
    e_ids = lax.broadcasted_iota(jnp.int32, (E, LANES), 0)
    lane_ids = lax.broadcasted_iota(jnp.int32, (E, LANES), 1)
    dz = z_me - (e_ids >> log2(p.x))
    dz = jnp.where(dz < 0, dz + p.z, dz)
    near = jnp.where(dz == 0, 0, jnp.where(2 * dz <= p.z, 2 * dz - 1, 2 * (p.z - dz)))
    my_place = near * p.x + ((x_me - (e_ids & (p.x - 1))) & (p.x - 1))
    my_lanes = (lane_ids >> log2(p.cap)) == (my_place & (p.per_chunk - 1))
    w_send[...] = jnp.where(my_lanes, spread, 0.0).reshape(E, 1, LANES)

    mark("barrier")
    pl.semaphore_wait(barrier, n_peers + p.tp - 1)
    mark("dispatch")

    for dz, dx in p.early():
        to = peer(dz, dx)
        at = p.place(-dz, -dx)
        remote(send_b.at[to], recv_b.at[at], disp_s, disp_r.at[at // p.per_chunk], (to, t)).start()
    for dz, dx in offsets:
        to = peer(dz, dx)
        at = p.place(-dz, -dx)
        remote(w_send.at[to], w_recv.at[at], wt_s, wt_r, (to, t)).start()
    recv_b[0] = send_b[me]
    w_recv[0] = w_send[me]
    by_token[...] = match.T.astype(BF)

    def move(k, way, a):
        r = (-(k - 1) if way == 0 else k - 1) % p.y
        to_r = (-k if way == 0 else k) % p.y
        copy = remote(
            g.at[r, c, a], g.at[to_r, c, a],
            ag_s.at[0 if k < p.half else 1], ag_r.at[way, k - 1, a], (me, ways[way]),
        )
        copy.start()

    def to_partner(r, a):
        piece = g.at[r, c, a]
        remote(piece, piece, pair_s, pair_r.at[r], (me, partner)).start()

    def from_partner(r):
        wait_for(g.at[r, 1 - c], pair_r.at[r])

    def lanes_of(r):
        return pl.ds(pl.multiple_of(lax.rem(y + r, p.y) * p.slab, p.slab), p.slab)

    def rows_of(r, kind):
        return jnp.concatenate(
            [
                jnp.concatenate([g[r, core, 2 * ch + kind] for ch in range(p.chunks)], axis=0)
                for core in range(2)
            ],
            axis=1,
        )

    def forward(r, first):
        from_partner(r)
        cols = lanes_of(r)
        up = dot(w_gu[:, cols], rows_of(r, 0), 1, 1)
        down = dot(w_dn[:, cols], rows_of(r, 1), 1, 1)
        if first:
            pre[...] = up
            back[...] = down
        else:
            pre[...] += up
            back[...] += down

    def arrive(u):
        mark(f"arrive{u}")
        arrived = p.per_chunk - (1 if u == 0 else 0)
        if arrived:
            wait_for(recv_b.at[pl.ds(0, arrived)], disp_r.at[u])
        both = recv_b[u * p.per_chunk : (u + 1) * p.per_chunk].astype(F32)
        g[0, c, 2 * u] = both[:, : p.cap].reshape(LANES, F).astype(BF)
        g[0, c, 2 * u + 1] = both[:, p.cap :].reshape(LANES, F).astype(BF)
        for a in (2 * u, 2 * u + 1):
            for way in range(2):
                if (u, a) in p.ring_units(1, way):
                    move(1, way, a)
        for a in (2 * u, 2 * u + 1):
            to_partner(0, a)

    def pass_on(k, u):
        mark(f"pass{k}{u}")
        for a in (2 * u, 2 * u + 1):
            for way in range(2):
                if (u, a) not in p.ring_units(k, way):
                    continue
                r = (-k if way == 0 else k) % p.y
                wait_for(g.at[r, c, a], ag_r.at[way, k - 1, a])
                if k < p.half and (u, a) in p.ring_units(k + 1, way):
                    move(k + 1, way, a)
                to_partner(r, a)

    def multiply(k):
        mark(f"multiply{k}")
        for r in sorted({k % p.y, -k % p.y}):
            forward(r, k == 0)

    for kind, k, u in p.gather_order():
        if kind == "arrive":
            arrive(u)
        elif kind == "pass":
            pass_on(k, u)
        else:
            if k == 0:
                for copy in loads:
                    copy.wait()
            multiply(k)
    wait_for(w_recv.at[pl.ds(0, n_peers)], wt_r)
    slot_weight = jnp.concatenate(
        [
            jnp.sum(w_recv[ch * p.per_chunk : (ch + 1) * p.per_chunk], axis=0)
            for ch in range(p.chunks)
        ],
        axis=1,
    )
    mark("hidden")

    part = jnp.zeros((1, S), F32)
    step = 32
    for b in range(0, H, step):
        pg, pu, bp = pre[b : b + step, :], pre[H + b : H + b + step, :], back[b : b + step, :]
        sig = lax.logistic(pg)
        act = pg * sig
        hid = act * pu
        part = part + jnp.sum(hid * bp, axis=0, keepdims=True)
        scaled[b : b + step, :] = (slot_weight * hid).astype(BF)
        hg = slot_weight * bp
        grads[b : b + step, :] = (hg * pu * sig * (1.0 + pg * (1.0 - sig))).astype(BF)
        grads[H + b : H + b + step, :] = (hg * act).astype(BF)
    for ch in range(p.chunks):
        g_part[ch : ch + 1, :] = part[:, ch * LANES : (ch + 1) * LANES]
    g_part[p.chunks :, :] = jnp.zeros((4 - p.chunks, LANES), F32)
    gp_recv[t] = g_part[...]
    grads_t[...] = grads[...].astype(F32).T.astype(BF)

    def slot_block(r):
        block = dot(grads_t[...], w_gu[:, lanes_of(r)])
        low, high = block[:, :F], block[:, F:]
        mine[r] = jnp.where(c == 0, low, high).astype(BF)
        p_send[r] = jnp.where(c == 0, high, low).astype(BF)
        remote(p_send.at[r], p_recv.at[r], ps_s, ps_r.at[r], (me, partner)).start()

    def chip_sum(r, u):
        if r not in ready:
            ready.add(r)
            wait_for(p_recv.at[r], ps_r.at[r])
        rows = pl.ds(u * p.unit_rows, p.unit_rows)
        return mine[r, rows].astype(F32) + p_recv[r, rows].astype(F32)

    def ring_send(way, u, d):
        r = (d if way == 0 else -d) % p.y
        total = chip_sum(r, u)
        longest = p.half if p.long_way(way, u) else p.half - 1
        if d < longest:
            wait_for(rs_r.at[way, u, d], rs_rs.at[way, u, d])
            total = total + rs_r[way, u, d].astype(F32)
        rs_s[way, u, d - 1] = total.astype(BF)
        remote(
            rs_s.at[way, u, d - 1], rs_r.at[way, u, d - 1],
            rs_ss.at[0 if p.long_way(way, u) else 1], rs_rs.at[way, u, d - 1], (me, ways[way]),
        ).start()

    def ring_step(j, long):
        for u in far + near:
            for way in range(2):
                d = p.half - j + (1 if long else 0)
                if p.long_way(way, u) == long and d >= 1:
                    ring_send(way, u, d)

    far, near = (3, 2), (1, 0)
    mark("ring1")
    order = [p.half]
    for d in range(p.half - 1, 0, -1):
        order += [d, p.y - d]
    order.append(0)
    ready = set()
    slot_block(order[0])
    for j in range(1, p.tp):
        remote(g_part, gp_recv.at[t], gp_s, gp_r, (me, lax.rem(t + j, p.tp))).start()
    for r in order[1:4]:
        slot_block(r)
    ring_step(1, True)
    for r in order[4:5]:
        slot_block(r)
    ring_step(1, False)
    for r in order[5:]:
        slot_block(r)

    mark("wgrads1")
    d_acc[...] = jnp.zeros_like(d_acc)

    def weight_grads(r):
        cols = lanes_of(r)
        both = dot(grads[...], rows_of(r, 0))
        dg[:, cols] = both[:H].astype(BF)
        du[:, cols] = both[H:].astype(BF)
        for row, part in enumerate((both[:H], both[H:])):
            square = jnp.sum(part * part, axis=0, keepdims=True)
            for core in range(2):
                sq[2 * lax.rem(y + r, p.y) + core, row : row + 1] = square[:, core * F : (core + 1) * F]
        down = dot(scaled[...], rows_of(r, 1))
        dd[:, cols] = down.astype(BF)
        square = down * down
        d_acc[...] += square[:, :F] + square[:, F:]

    slabs = list(range(p.y))
    per_step = -(-p.y // max(1, p.half - 1)) if p.half > 1 else p.y

    def gate_sum():
        wait_for(gp_recv.at[pl.ds(0, p.tp - 1)], gp_r)
        total = jnp.sum(gp_recv[...], axis=0)
        for ch in range(p.chunks):
            g_send[ch] = total[ch : ch + 1, :]
        for dz, dx in offsets:
            to = peer(dz, dx)
            row = p.place(dz, dx) // p.per_chunk
            remote(g_send.at[row], g_recv.at[me], gc_s, gc_r, (to, t)).start()
        g_recv[me] = g_send[0]

    def send_squares():
        for j in range(1, p.tp):
            to = lax.rem(t + j, p.tp)
            remote(sq.at[to], sq_recv.at[t], sq_s, sq_r, (me, to)).start()
        sq_recv[t] = sq[t]

    for j in range(2, p.half + 1):
        for r in slabs[:per_step]:
            weight_grads(r)
        slabs = slabs[per_step:]
        mark(f"ring{j}")
        ring_step(j, True)
        mark(f"ring{j}b")
        ring_step(j, False)
        if j == 2:
            mark("gate_sum")
            gate_sum()
        mark(f"wgrads{j}")
        if j == p.half - 1 and j > 1:
            for r in slabs:
                weight_grads(r)
            slabs = []
            send_squares()
    for r in slabs:
        weight_grads(r)
    if p.half < 3:
        send_squares()
    if p.half < 2:
        gate_sum()
    mark("last_ring")
    def finish(u):
        total = chip_sum(0, u)
        for way in range(2):
            if p.half > 1 or p.long_way(way, u):
                wait_for(rs_r.at[way, u, 0], rs_rs.at[way, u, 0])
                total = total + rs_r[way, u, 0].astype(F32)
        block[u] = total
        if p.unit_rows % p.cap == 0:
            per = p.unit_rows // p.cap
            c_buf[u * per : (u + 1) * per] = total.reshape(per, p.cap, F).astype(BF)
            sources = range(u * per, (u + 1) * per)
        elif len(block) == p.units:
            whole = jnp.concatenate([block[v] for v in range(p.units)], axis=0)
            c_buf[...] = whole.reshape(E, p.cap, F).astype(BF)
            sources = range(E)
        else:
            sources = ()
        for dz, dx in offsets:
            if p.place(dz, dx) in sources:
                to = peer(dz, dx)
                remote(c_buf.at[p.place(dz, dx)], c_recv.at[me], cb_s, cb_r, (to, t)).start()

    block = {}
    for u in far:
        finish(u)
    mark("gate")
    wait_for(g_recv.at[pl.ds(0, n_peers)], gc_r)
    kept = jnp.where(my_lanes, g_recv[...].reshape(E, LANES), 0.0)
    picked = dot(kept, hits[...], 0, 0, HI)
    lane_twice = jnp.concatenate([lane_slot, lane_slot], axis=1)
    gates = jnp.sum(jnp.where(lane_twice == places[...], picked, 0.0), axis=0, keepdims=True)
    gate = [gates[:, k * T : (k + 1) * T] for k in range(2)]
    for k in range(2):
        gate_out[k : k + 1, :] = gate[k]
    mixed = weights[0:1, :] * gate[0] + weights[1:2, :] * gate[1]
    logit = [weights[k : k + 1, :] * (gate[k] - mixed) for k in range(2)]
    signal = (hits[:, :T] * logit[0] + hits[:, T:] * logit[1]).astype(BF)
    rt_send[...] = dot(signal, tokens).reshape(E, 1, F)
    for dz, dx in offsets:
        to = peer(dz, dx)
        remote(rt_send.at[to], rt_recv.at[me], rt_s, rt_r, (to, t)).start()
    rt_recv[me] = rt_send[me]
    mark("finish")
    for u in near:
        finish(u)
    c_recv[me] = c_buf[0]
    wait_for(sq_recv.at[pl.ds(0, p.tp - 1)], sq_r)
    sq_sum[...] = jnp.sum(sq_recv[...], axis=0) * (1.0 / (H * p.tp))
    for j in range(1, p.tp):
        remote(sq_sum, sq_all.at[t], sa_s, sa_r, (me, lax.rem(t + j, p.tp))).start()
    sq_all[t] = sq_sum[...]
    from_router = dot(signal.astype(F32).T.astype(BF), r_cols[...])
    ones = jnp.ones((8, F), F32)
    dsq_out[...] = dot(ones, d_acc[...], 1, 1, HI)[0:1, :] * (1.0 / p.features)

    mark("token")
    wait_for(c_recv.at[pl.ds(0, n_peers)], cb_r)
    rows = c_recv[...].astype(F32).reshape(S, F).astype(BF)
    token_out[...] = dot(by_token[...], rows) + from_router
    mark("router")
    wait_for(rt_recv.at[pl.ds(0, n_peers)], rt_r)
    router_out[...] = jnp.sum(rt_recv[...], axis=0)
    mark("squares")
    wait_for(sq_all.at[pl.ds(0, p.tp - 1)], sa_r)
    for i in range(p.tp):
        gsq_out[:, i * F : (i + 1) * F] = sq_all[i, 0:1]
        usq_out[:, i * F : (i + 1) * F] = sq_all[i, 1:2]

    mark("sends")
    if p.half > 1:
        wait_for(g.at[pl.ds(0, p.half - 1)], ag_s.at[0])
        wait_for(rs_s.at[0, :, pl.ds(0, p.half - 1)], rs_ss.at[1])
    wait_for(g.at[0, 0], ag_s.at[1])
    wait_for(rs_s.at[0], rs_ss.at[0])
    wait_for(g.at[pl.ds(0, p.half)], pair_s)
    wait_for(p_recv, ps_s)
    wait_for(send_b.at[pl.ds(0, n_peers)], disp_s)
    wait_for(w_send.at[pl.ds(0, n_peers)], wt_s)
    wait_for(gp_recv.at[pl.ds(0, p.tp - 1)], gp_s)
    wait_for(g_recv.at[pl.ds(0, n_peers)], gc_s)
    wait_for(c_recv.at[pl.ds(0, n_peers)], cb_s)
    wait_for(rt_recv.at[pl.ds(0, n_peers)], rt_s)
    wait_for(sq_recv.at[pl.ds(0, p.tp - 1)], sq_s)
    wait_for(sq_all.at[pl.ds(0, p.tp - 1)], sa_s)
    mark(None)


def run(p, routing, weights, tokens, cotangent, gate_t, up_t, down, router_t):
    H, S, E, T, F, D, N = p.hidden, p.slots, p.ep, p.tok, p.width, p.features, p.tp
    vm, hbm = pl.BlockSpec(memory_space=pltpu.VMEM), pl.BlockSpec(memory_space=pltpu.HBM)
    V, dma = pltpu.VMEM, pltpu.SemaphoreType.DMA
    scratch = [
        V((2, T), jnp.int32), V((2, T), BF), V((T, F), BF), V((T, F), BF),
        V((2 * H, D), BF), V((H, D), BF), V((E, F), BF),
        V((E, 2 * p.cap, F), BF), V((E, 2 * p.cap, F), BF),
        V((E, 1, LANES), F32), V((E, 1, LANES), F32),
        V((T, S), BF), V((E, 2 * T), F32), V((1, 2 * T), F32),
        V((p.y, 2, 2 * p.chunks, LANES, F), BF),
        V((2 * H, S), F32), V((H, S), F32), V((2 * H, S), BF), V((S, 2 * H), BF), V((H, S), BF),
        V((4, LANES), F32), V((N, 4, LANES), F32), V((p.chunks, 1, LANES), F32), V((E, 1, LANES), F32),
        V((p.y, S, F), BF), V((p.y, S, F), BF), V((p.y, S, F), BF),
        V((2, p.units, p.half, p.unit_rows, F), BF), V((2, p.units, p.half, p.unit_rows, F), BF),
        V((E, p.cap, F), BF), V((E, p.cap, F), BF),
        V((E, 1, F), F32), V((E, 1, F), F32),
        V((N, 2, F), F32), V((N, 2, F), F32), V((2, F), F32), V((N, 2, F), F32),
        V((H, F), F32),
        dma((8,)), dma, dma((p.chunks,)), dma, dma,
        dma((2,)), dma((2, p.half, 2 * p.chunks)),
        dma, dma((p.y,)),
        dma, dma, dma, dma,
        dma, dma((p.y,)),
        dma((2,)), dma((2, p.units, p.half)),
        dma, dma, dma, dma, dma, dma, dma, dma,
    ]
    shape = jax.ShapeDtypeStruct
    shapes = (
        shape((T, F), F32), shape((2, T), F32),
        shape((H, D), BF), shape((H, D), BF), shape((H, D), BF),
        shape((1, F), F32), shape((1, D), F32), shape((1, D), F32), shape((1, H), F32),
    )
    results = pl.pallas_call(
        functools.partial(kernel, p),
        out_shape=shapes,
        in_specs=[hbm] * 8,
        out_specs=(vm,) * len(shapes),
        scratch_shapes=scratch,
        compiler_params=pltpu.CompilerParams(
            collective_id=0, has_side_effects=True, vmem_limit_bytes=40 << 20
        ),
        name="expert_backward",
    )(*(
        pltpu.with_memory_space_constraint(a, pltpu.HBM)
        for a in (routing, weights, tokens, cotangent, gate_t, up_t, down, router_t)
    ))
    return pl.pallas_call(
        store,
        out_shape=shapes,
        in_specs=[vm] * len(shapes),
        out_specs=(hbm,) * len(shapes),
        scratch_shapes=[dma((len(shapes),))],
        compiler_params=pltpu.CompilerParams(vmem_limit_bytes=1 << 20),
        name="store_results",
    )(*results)


def store(*refs):
    n = len(refs) // 2
    copies = [pltpu.make_async_copy(refs[i], refs[n + i], refs[-1].at[i]) for i in range(n)]
    for copy in copies:
        copy.start()
    for copy in copies:
        copy.wait()


def shards(tokens, routing, gate_weights, cotangent, expert_gate, expert_up, expert_down, router):
    tok, width = tokens.shape
    n_ep, n_tp = lax.axis_size("ep"), lax.axis_size("tp")
    experts = router.shape[1]
    cap = 3 * routing.shape[1] * tok // (2 * experts)
    p = Plan(n_ep, n_tp, tok, width, expert_gate.shape[2], width * n_tp, cap)
    out = run(
        p, routing.T, gate_weights.T, tokens, cotangent,
        expert_gate[0].T, expert_up[0].T, expert_down[0], router.T,
    )
    token_grad, gate_grad, dgate, dup, ddown, router_grad, gsq, usq, dsq = out
    return (
        token_grad, gate_grad.T, dgate.T[None], dup.T[None], ddown[None], router_grad, gsq, usq, dsq,
    )


def solution(mesh):
    in_specs = (
        P("ep", "tp"),
        P("ep", None),
        P("ep", None),
        P("ep", "tp"),
        P("ep", None, "tp"),
        P("ep", None, "tp"),
        P("ep", "tp", None),
        P(),
    )
    out_specs = (
        P("ep", "tp"),
        P("ep", None),
        P("ep", None, "tp"),
        P("ep", None, "tp"),
        P("ep", "tp", None),
        P("ep", "tp"),
        P("ep", None),
        P("ep", None),
        P("ep", "tp"),
    )
    return jax.shard_map(shards, mesh=mesh, in_specs=in_specs, out_specs=out_specs, check_vma=False)
```

time: 91.4 us -> 73.4 us (0.80)
  local copies, waits for them, and re-layouts: 12.6 us -> 0 us
  Pallas kernels: 77.6 us -> 72.5 us
    unnamed x25 -> x0, local copies, waits for them, and re-layouts: 12.6 us -> none
    pallas_call x1 -> x2, Pallas kernels: 77.6 us -> 72.5 us  [the longest x1 71 us: run(): pl.pallas_call(functools.partial(kernel, p), out_shape=shapes, in_specs=[...]
where the time goes in v2:
time: 73.4 us; the launch traced here: 73.2 us
  Pallas kernels  72.5 us (99%)
    pallas_call x1, Pallas kernels, run(): pl.pallas_call(functools.partial(kernel, p), out_shape=shapes, in_specs=[...  71 us
    pallas_call x1, Pallas kernels, run(): pl.pallas_call(store, out_shape=shapes, in_specs=[vm] * len(shapes), out_...  1.52 us

profile of v2, /device:TPU:1, one launch (start us, length us, event | category | flops | bytes accessed | tf_op | source)
XLA Modules:
  0.0 73.2 jit_solution(10197326577197868560)
XLA Ops:
  0.6 71.0 %expert_backward.1 = (f32[128,128]{1,0:T(8,128)S(1)}, f32[2,128]{1,0:T(2,128)S(1)}, bf16[192,2048]{1,0:T(8,128)(2,1)S(1)}, bf16[192,2048]{1,0:T(8,128)(2,1)S(1)}...) custom-call(s32[2,128]{1,0:T(2,128)} %bitcast.22, ...), custom_call_target="tpu_custom_call" | custom-call | tf_op jit(solution)/shard_map/expert_backward/pallas_call | solution.py:557
  71.7 1.5 %store_results.1 = (f32[128,128]{1,0:T(8,128)}, f32[2,128]{1,0:T(2,128)}, bf16[192,2048]{1,0:T(8,128)(2,1)}, bf16[192,2048]{1,0:T(8,128)(2,1)}, bf16[192,2048]{1...) custom-call(f32[128,128]{1,0:T(8,128)S(1)} %get-tuple-element.27.refs_0_, ...), custom_call_target="tpu_custom_call" | custom-call | tf_op jit(solution)/shard_map/store_results/pallas_call | solution.py:571

commit v3 on v2

--- a/solution.py
+++ b/solution.py
@@ -47,7 +47,7 @@
         self.slots = n_ep * cap
         self.chunks = self.slots // LANES
         self.per_chunk = LANES // cap
-        self.units = 4
+        self.units = 6
         self.unit_rows = self.slots // self.units
         self.slab = 2 * width
 
@@ -80,8 +80,8 @@
             a, p, m = "arrive", "pass", "multiply"
             return (
                 (a, 0, 0), (a, 0, 1), (p, 1, 0), (a, 0, 2), (p, 1, 1), (p, 2, 0), (p, 1, 2),
-                (p, 2, 1), (m, 0, 0), (p, 3, 0), (p, 2, 2), (p, 3, 1), (m, 1, 0), (p, 4, 0),
-                (p, 3, 2), (m, 2, 0), (p, 4, 1), (p, 4, 2), (m, 3, 0), (m, 4, 0),
+                (p, 2, 1), (m, 0, 0), (p, 2, 2), (p, 3, 0), (m, 1, 0), (p, 3, 1), (p, 3, 2),
+                (p, 4, 0), (m, 2, 0), (p, 4, 1), (p, 4, 2), (m, 3, 0), (m, 4, 0),
             )
         out = [("arrive", 0, u) for u in range(self.chunks)] + [("multiply", 0, 0)]
         for k in range(1, self.half + 1):
@@ -114,6 +114,7 @@
     right = lax.rem(y + 1, p.y) * 2 + c
     left = lax.rem(y + p.y - 1, p.y) * 2 + c
     ways = (right, left)
+    other_ways = (right + 1 - 2 * c, left + 1 - 2 * c)
     H, S, E, T, F = p.hidden, p.slots, p.ep, p.tok, p.width
 
     def peer(dz, dx):
@@ -202,12 +203,7 @@
         to = peer(dz, dx)
         at = p.place(-dz, -dx)
         remote(send_b.at[to], recv_b.at[at], disp_s, disp_r.at[at // p.per_chunk], (to, t)).start()
-    for dz, dx in offsets:
-        to = peer(dz, dx)
-        at = p.place(-dz, -dx)
-        remote(w_send.at[to], w_recv.at[at], wt_s, wt_r, (to, t)).start()
     recv_b[0] = send_b[me]
-    w_recv[0] = w_send[me]
     by_token[...] = match.T.astype(BF)
 
     def move(k, way, a):
@@ -218,6 +214,9 @@
             ag_s.at[0 if k < p.half else 1], ag_r.at[way, k - 1, a], (me, ways[way]),
         )
         copy.start()
+
+    def both_cores(k, a):
+        return k == p.half and k > 1 and a // 2 == p.chunks - 1
 
     def to_partner(r, a):
         piece = g.at[r, c, a]
@@ -265,6 +264,13 @@
         for a in (2 * u, 2 * u + 1):
             to_partner(0, a)
 
+    def send_weights():
+        for dz, dx in offsets:
+            to = peer(dz, dx)
+            at = p.place(-dz, -dx)
+            remote(w_send.at[to], w_recv.at[at], wt_s, wt_r, (to, t)).start()
+        w_recv[0] = w_send[me]
+
     def pass_on(k, u):
         mark(f"pass{k}{u}")
         for a in (2 * u, 2 * u + 1):
@@ -275,7 +281,13 @@
                 wait_for(g.at[r, c, a], ag_r.at[way, k - 1, a])
                 if k < p.half and (u, a) in p.ring_units(k + 1, way):
                     move(k + 1, way, a)
-                to_partner(r, a)
+                    if both_cores(k + 1, a):
+                        remote(
+                            g.at[r, c, a], g.at[p.half, c, a],
+                            pair_s, pair_r.at[p.half], (me, other_ways[way]),
+                        ).start()
+                if not both_cores(k, a):
+                    to_partner(r, a)
 
     def multiply(k):
         mark(f"multiply{k}")
@@ -285,6 +297,8 @@
     for kind, k, u in p.gather_order():
         if kind == "arrive":
             arrive(u)
+            if u == p.chunks - 1:
+                send_weights()
         elif kind == "pass":
             pass_on(k, u)
         else:
@@ -354,7 +368,8 @@
                 if p.long_way(way, u) == long and d >= 1:
                     ring_send(way, u, d)
 
-    far, near = (3, 2), (1, 0)
+    backward = tuple(range(p.units))[::-1]
+    far, near = backward[: p.units // 2], backward[p.units // 2 :]
     mark("ring1")
     order = [p.half]
     for d in range(p.half - 1, 0, -1):
@@ -391,7 +406,6 @@
         d_acc[...] += square[:, :F] + square[:, F:]
 
     slabs = list(range(p.y))
-    per_step = -(-p.y // max(1, p.half - 1)) if p.half > 1 else p.y
 
     def gate_sum():
         wait_for(gp_recv.at[pl.ds(0, p.tp - 1)], gp_r)
@@ -410,29 +424,30 @@
             remote(sq.at[to], sq_recv.at[t], sq_s, sq_r, (me, to)).start()
         sq_recv[t] = sq[t]
 
+    counts = {1: 3, 2: 2, 3: 3} if p.half == 4 else {}
+    for r in slabs[: counts.get(1, 0)]:
+        weight_grads(r)
+    slabs = slabs[counts.get(1, 0) :]
     for j in range(2, p.half + 1):
-        for r in slabs[:per_step]:
-            weight_grads(r)
-        slabs = slabs[per_step:]
         mark(f"ring{j}")
         ring_step(j, True)
-        mark(f"ring{j}b")
-        ring_step(j, False)
         if j == 2:
             mark("gate_sum")
             gate_sum()
+        mark(f"ring{j}b")
+        ring_step(j, False)
         mark(f"wgrads{j}")
-        if j == p.half - 1 and j > 1:
-            for r in slabs:
-                weight_grads(r)
-            slabs = []
+        for r in slabs[: counts.get(j, 0)]:
+            weight_grads(r)
+        slabs = slabs[counts.get(j, 0) :]
+        if j == max(counts, default=0):
             send_squares()
+    if p.half < 2:
+        gate_sum()
     for r in slabs:
         weight_grads(r)
-    if p.half < 3:
+    if not counts:
         send_squares()
-    if p.half < 2:
-        gate_sum()
     mark("last_ring")
     def finish(u):
         total = chip_sum(0, u)
@@ -480,15 +495,15 @@
     for u in near:
         finish(u)
     c_recv[me] = c_buf[0]
+    from_router = dot(signal.astype(F32).T.astype(BF), r_cols[...])
+    ones = jnp.ones((8, F), F32)
+    dsq_out[...] = dot(ones, d_acc[...], 1, 1, HI)[0:1, :] * (1.0 / p.features)
+
     wait_for(sq_recv.at[pl.ds(0, p.tp - 1)], sq_r)
     sq_sum[...] = jnp.sum(sq_recv[...], axis=0) * (1.0 / (H * p.tp))
     for j in range(1, p.tp):
         remote(sq_sum, sq_all.at[t], sa_s, sa_r, (me, lax.rem(t + j, p.tp))).start()
     sq_all[t] = sq_sum[...]
-    from_router = dot(signal.astype(F32).T.astype(BF), r_cols[...])
-    ones = jnp.ones((8, F), F32)
-    dsq_out[...] = dot(ones, d_acc[...], 1, 1, HI)[0:1, :] * (1.0 / p.features)
-
     mark("token")
     wait_for(c_recv.at[pl.ds(0, n_peers)], cb_r)
     rows = c_recv[...].astype(F32).reshape(S, F).astype(BF)

time: 73.4 us -> 73.2 us (level)
  no operation moved by 1% of the time
where the time goes in v3:
time: 73.2 us; the launch traced here: 73 us
  Pallas kernels  72.3 us (99%)
    pallas_call x1, Pallas kernels, run(): pl.pallas_call(functools.partial(kernel, p), out_shape=shapes, in_specs=[...  70.8 us
    pallas_call x1, Pallas kernels, run(): pl.pallas_call(store, out_shape=shapes, in_specs=[vm] * len(shapes), out_...  1.52 us

profile of v3, /device:TPU:1, one launch (start us, length us, event | category | flops | bytes accessed | tf_op | source)
XLA Modules:
  0.0 73.0 jit_solution(7634168713214002845)
XLA Ops:
  0.6 70.8 %expert_backward.1 = (f32[128,128]{1,0:T(8,128)S(1)}, f32[2,128]{1,0:T(2,128)S(1)}, bf16[192,2048]{1,0:T(8,128)(2,1)S(1)}, bf16[192,2048]{1,0:T(8,128)(2,1)S(1)}...) custom-call(s32[2,128]{1,0:T(2,128)} %bitcast.22, ...), custom_call_target="tpu_custom_call" | custom-call | tf_op jit(solution)/shard_map/expert_backward/pallas_call | solution.py:572
  71.5 1.5 %store_results.1 = (f32[128,128]{1,0:T(8,128)}, f32[2,128]{1,0:T(2,128)}, bf16[192,2048]{1,0:T(8,128)(2,1)}, bf16[192,2048]{1,0:T(8,128)(2,1)}, bf16[192,2048]{1...) custom-call(f32[128,128]{1,0:T(8,128)S(1)} %get-tuple-element.27.refs_0_, ...), custom_call_target="tpu_custom_call" | custom-call | tf_op jit(solution)/shard_map/store_results/pallas_call | solution.py:586
